TPU v7x, 32 devices: a whole 2x2x4 slice. The times are simulated.
32 devices in a mesh: ra: 8 (over z, y), cb: 4 (over x, core).
Axes of the slice: x: 2, y: 2, z: 4, core: 2. Of those that a mesh axis runs over, the one named last changes fastest.
Arguments:
- activations: bfloat16 [512, 4224], P('cb', 'ra'), may hold values from -160 to 160, as said below
- norm_gain: float32 [2, 4224], replicated, may hold values from 0.1 to 1.9
- gate_weight: float32 [2, 4224, 11520], P(None, None, 'ra'), may hold values from -0.09375 to 0.09375
- gate_scale: float32 [2, 11520], P(None, 'ra'), may hold values from 0.3 to 3
- value_weight: float32 [2, 4224, 11520], P(None, None, 'ra'), may hold values from -0.09375 to 0.09375
- value_scale: float32 [2, 11520], P(None, 'ra'), may hold values from 0.3 to 3
- gate_taps: float32 [2, 3, 11520], P(None, None, 'ra'), may hold values from -3 to 3
- value_taps: float32 [2, 3, 11520], P(None, None, 'ra'), may hold values from -3 to 3
- down_weight: float32 [2, 11520, 4224], P(None, None, 'ra'), may hold values from -0.0546875 to 0.0546875
- down_scale: float32 [2, 4224], P(None, 'ra'), may hold values from 0.3 to 3
- final_gain: float32 [4224], P('ra'), may hold values from 0.1 to 1.9
Outputs:
- normalized: bfloat16 [512, 4224], P('cb', 'ra')
Inputs may be any that keep to these rules, and one draw needn't show every extreme that they name: `activations`: rows and columns have unequal scales.
All inputs are finite; a program needn't handle non-finite values.
Results may differ from a plain program's by a relative error of at most 0.017.
Values may be sent and summed in bfloat16 or wider, within the bound.
A program may use at most 320 MiB of HBM per device.

v0:
```python
import jax
import jax.numpy as jnp
from jax import lax
from jax.sharding import PartitionSpec as P

D = 4224
epsilon = 1e-06
resid_scale = 0.5


def from_behind(value, axis, by):
    length = lax.axis_size(axis)
    pairs = [(i, i + by) for i in range(length) if 0 <= i + by < length]
    return lax.ppermute(value, axis, pairs)


def conv_local(values_in, earlier, tap_weights):
    seq_len = values_in.shape[0]
    taps = tap_weights.shape[0]
    padded = jnp.concatenate([earlier, values_in], axis=0)
    total = jnp.zeros(values_in.shape, jnp.float32)
    for offset in range(taps):
        total = total + tap_weights[offset] * padded[offset : offset + seq_len]
    return total


def per_device(
    activations,
    norm_gain,
    gate_weight,
    gate_scale,
    value_weight,
    value_scale,
    gate_taps,
    value_taps,
    down_weight,
    down_scale,
    final_gain,
):
    row_count, width_part = activations.shape
    tok_rows = activations
    layer_count = gate_weight.shape[0]
    taps = gate_taps.shape[1]
    for layer_idx in range(layer_count):
        wide_rows = tok_rows.astype(jnp.float32)
        full_rows = lax.all_gather(tok_rows, "ra", axis=1, tiled=True).astype(jnp.float32)
        inv_norm = lax.rsqrt(jnp.mean(full_rows * full_rows, axis=1, keepdims=True) + epsilon)
        scaled = (full_rows * norm_gain[layer_idx]).astype(jnp.bfloat16)
        gate_pre = (
            jnp.dot(
                scaled,
                gate_weight[layer_idx].astype(jnp.bfloat16),
                preferred_element_type=jnp.float32,
            )
            * inv_norm
            * gate_scale[layer_idx]
        )
        value_pre = (
            jnp.dot(
                scaled,
                value_weight[layer_idx].astype(jnp.bfloat16),
                preferred_element_type=jnp.float32,
            )
            * inv_norm
            * value_scale[layer_idx]
        )
        gate_prev, value_prev = from_behind(
            (gate_pre[row_count - taps + 1 :], value_pre[row_count - taps + 1 :]), "cb", 1
        )
        gate_conv = conv_local(gate_pre, gate_prev, gate_taps[layer_idx])
        value_conv = conv_local(value_pre, value_prev, value_taps[layer_idx])
        down_bf = down_weight[layer_idx].astype(jnp.bfloat16)
        hidden = (jax.nn.silu(gate_conv) * value_conv).astype(jnp.bfloat16)
        down = jnp.dot(
            lax.all_gather(hidden, "ra", axis=1, tiled=True),
            down_bf,
            preferred_element_type=jnp.float32,
        )
        tok_rows = (resid_scale * wide_rows + down * down_scale[layer_idx]).astype(jnp.bfloat16)
    wide_rows = tok_rows.astype(jnp.float32)
    sq_final = lax.psum(jnp.sum(wide_rows * wide_rows, axis=1), "ra")
    inv_norm = lax.rsqrt(sq_final[:, None] / D + epsilon)
    return (wide_rows * inv_norm * final_gain).astype(jnp.bfloat16)


def solution(mesh):
    in_specs = (
        P("cb", "ra"),
        P(),
        P(None, None, "ra"),
        P(None, "ra"),
        P(None, None, "ra"),
        P(None, "ra"),
        P(None, None, "ra"),
        P(None, None, "ra"),
        P(None, None, "ra"),
        P(None, "ra"),
        P("ra"),
    )
    out_specs = P("cb", "ra")
    return jax.shard_map(
        per_device, mesh=mesh, in_specs=in_specs, out_specs=out_specs, check_vma=False
    )
```

profile of v0, /device:TPU:0, one launch (start us, length us, event | category | flops | bytes accessed | tf_op | source)
XLA Modules:
  0.0 316.4 jit_solution(9558296523419066182)
XLA Ops:
  6.5 0.7 all-gather.5.cloned.1.call-update
  7.3 24.9 %convert.12 = bf16[2,4224,1440]{1,2,0:T(8,128)(2,1)} convert(f32[2,4224,1440]{1,2,0:T(8,128)} %param.13) | non-fusion elementwise | flops 12165120 | bytes 72990720 | tf_op jit(solution)/shard_map/convert.5
  32.2 24.9 %convert.13 = bf16[2,4224,1440]{1,2,0:T(8,128)(2,1)} convert(f32[2,4224,1440]{1,2,0:T(8,128)} %param.15) | non-fusion elementwise | flops 12165120 | bytes 72990720 | tf_op jit(solution)/shard_map/convert.4
  57.3 1.8 fusion.15
  59.1 8.2 %fusion.13 = f32[128,1440]{0,1:T(8,128)S(1)} fusion(bf16[2,4224,1440]{1,2,0:T(8,128)(2,1)} %convert.12, bf16[128,4224]{0,1:T(8,128)(2,1)} %all-gather.5.cloned.1.call-done, f32[4224]{0:T(1024)S(1)} %get-tuple-element.18, f32[1440]{0:T(1024)S(1)} %get-tuple-element.20, f32[128]{0:T(128)S(1)} %add_rsqrt_fusion.2), kind=kOutput, calls=%fused_computation.23 | convolution fusion | flops 1559126016 | bytes 14006912 | tf_op jit(solution)/shard_map/dot_general | solution.py:50
  67.9 2.4 collective-permute-start
  70.3 8.0 %fusion.12 = f32[128,1440]{0,1:T(8,128)S(1)} fusion(bf16[2,4224,1440]{1,2,0:T(8,128)(2,1)} %convert.13, bf16[128,4224]{0,1:T(8,128)(2,1)S(1)} %copy-done, f32[4224]{0:T(1024)S(1)} %get-tuple-element.18, f32[1440]{0:T(1024)S(1)} %get-tuple-element.22, f32[128]{0:T(128)S(1)} %add_rsqrt_fusion.2), kind=kOutput, calls=%fused_computation.22 | convolution fusion | flops 1559126016 | bytes 14006912 | tf_op jit(solution)/shard_map/dot_general | solution.py:59
  78.8 4.5 %collective-permute-start.1 = (f32[2,1440]{1,0:T(2,128)S(1)}, f32[2,1440]{1,0:T(2,128)S(1)}, u32[]{:S(2)}, u32[]{:S(2)}) collective-permute-start(f32[2,1440]{1,0:T(2,128)S(1)} %copy.14), channel_id=1, source_target_pairs={{0,1},{1,2},{2,3},{4,5},{5,6},{6,7},{8,9},{9,10},{10,11},{12,13},{... | collective-permute-start | bytes 34568 | tf_op jit(solution)/shard_map/ppermute | solution.py:14
  84.4 3.3 %fusion.40 = bf16[128,1440]{0,1:T(8,128)(2,1)} fusion(f32[2,1440]{0,1:T(8,128)S(1)} %copy.15, f32[128,1440]{0,1:T(8,128)S(1)} %fusion.12, f32[128,1440]{0,1:T(8,128)S(1)} %fusion.13, f32[2,1440]{0,1:T(8,128)S(1)} %copy.13, f32[1440]{0:T(1024)S(1)} %get-tuple-element.12, f32[1440]{0:T(1024)S(1)} %get-tuple-element.13, f32[1440]{0:T(1024)S(1)} %get-tuple-element.14, ...), kind=kLoop, calls=%fused_computation.58 | loop fusion | flops 3686400 | bytes 1900800 | tf_op jit(solution)/shard_map/convert_element_type | solution.py:73
  87.8 25.0 %convert.14 = bf16[2,11520,528]{1,2,0:T(8,128)(2,1)} convert(f32[2,11520,528]{1,2,0:T(8,128)} %param.19) | non-fusion elementwise | flops 12165120 | bytes 72990720 | tf_op jit(solution)/shard_map/convert.3
  112.8 34.9 %all-gather.7.cloned.1.call-done = bf16[128,11520]{0,1:T(8,128)(2,1)} async-done(((bf16[128,1440]{0,1:T(8,128)(2,1)}), bf16[128,11520]{0,1:T(8,128)(2,1)}) %all-gather.7.cloned.1.call-update) | async-done | bytes 2949136 | tf_op jit(solution)/shard_map/all_gather | solution.py:75
  147.7 9.3 %fusion.24 = bf16[128,528]{0,1:T(8,128)(2,1)} fusion(bf16[128,11520]{0,1:T(8,128)(2,1)} %all-gather.7.cloned.1.call-done, bf16[2,11520,528]{1,2,0:T(8,128)(2,1)} %convert.14, bf16[128,528]{0,1:T(8,128)(2,1)S(1)} %copy-done.2, f32[528]{0:T(1024)S(1)} %get-tuple-element.24), kind=kOutput, calls=%fused_computation.42 | convolution fusion | flops 1557473280 | bytes 15386688 | tf_op jit(solution)/shard_map/dot_general | solution.py:74
  157.2 39.1 %all-gather.9.cloned.1.call-done = bf16[128,4224]{0,1:T(8,128)(2,1)} async-done(((bf16[128,528]{0,1:T(8,128)(2,1)}), bf16[128,4224]{0,1:T(8,128)(2,1)}) %all-gather.9.cloned.1.call-update) | async-done | bytes 1081360 | tf_op jit(solution)/shard_map/all_gather | solution.py:46
  196.3 1.8 fusion.17
  198.1 8.2 %fusion.11 = f32[128,1440]{0,1:T(8,128)S(1)} fusion(bf16[2,4224,1440]{1,2,0:T(8,128)(2,1)} %convert.12, bf16[128,4224]{0,1:T(8,128)(2,1)} %all-gather.9.cloned.1.call-done, f32[4224]{0:T(1024)S(1)} %get-tuple-element.17, f32[1440]{0:T(1024)S(1)} %get-tuple-element.19, f32[128]{0:T(128)S(1)} %add_rsqrt_fusion.1), kind=kOutput, calls=%fused_computation.21 | convolution fusion | flops 1559126016 | bytes 14006912 | tf_op jit(solution)/shard_map/dot_general | solution.py:50
  206.9 1.3 collective-permute-start.2
  208.2 8.0 %fusion.10 = f32[128,1440]{0,1:T(8,128)S(1)} fusion(bf16[2,4224,1440]{1,2,0:T(8,128)(2,1)} %convert.13, bf16[128,4224]{0,1:T(8,128)(2,1)S(1)} %copy-done.1, f32[4224]{0:T(1024)S(1)} %get-tuple-element.17, f32[1440]{0:T(1024)S(1)} %get-tuple-element.21, f32[128]{0:T(128)S(1)} %add_rsqrt_fusion.1), kind=kOutput, calls=%fused_computation.20 | convolution fusion | flops 1559126016 | bytes 14006912 | tf_op jit(solution)/shard_map/dot_general | solution.py:59
  216.7 4.1 %collective-permute-start.3 = (f32[2,1440]{1,0:T(2,128)S(1)}, f32[2,1440]{1,0:T(2,128)S(1)}, u32[]{:S(2)}, u32[]{:S(2)}) collective-permute-start(f32[2,1440]{1,0:T(2,128)S(1)} %copy.18), channel_id=1, source_target_pairs={{0,1},{1,2},{2,3},{4,5},{5,6},{6,7},{8,9},{9,10},{10,11},{12,13},{... | collective-permute-start | bytes 34568 | tf_op jit(solution)/shard_map/ppermute | solution.py:14
  221.1 0.5 collective-permute-done.3
  221.9 3.3 %fusion.30 = bf16[128,1440]{0,1:T(8,128)(2,1)} fusion(f32[2,1440]{0,1:T(8,128)S(1)} %copy.19, f32[128,1440]{0,1:T(8,128)S(1)} %fusion.10, f32[128,1440]{0,1:T(8,128)S(1)} %fusion.11, f32[2,1440]{0,1:T(8,128)S(1)} %copy.17, f32[1440]{0:T(1024)S(1)} %get-tuple-element.15, f32[1440]{0:T(1024)S(1)} %get-tuple-element.16, f32[1440]{0:T(1024)S(1)} %get-tuple-element.11, ...), kind=kLoop, calls=%fused_computation.48 | loop fusion | flops 3686400 | bytes 1900800 | tf_op jit(solution)/shard_map/convert_element_type | solution.py:73
  225.2 57.5 %all-gather.11.cloned.1.call-done = bf16[128,11520]{0,1:T(8,128)(2,1)} async-done(((bf16[128,1440]{0,1:T(8,128)(2,1)}), bf16[128,11520]{0,1:T(8,128)(2,1)}) %all-gather.11.cloned.1.call-update) | async-done | bytes 2949136 | tf_op jit(solution)/shard_map/all_gather | solution.py:75
  282.7 7.2 %multiply_reduce_fusion = (f32[128]{0:T(128)S(1)}, f32[128,528]{0,1:T(8,128)S(1)}) fusion(f32[528]{0:T(1024)S(1)} %get-tuple-element.23, bf16[128,11520]{0,1:T(8,128)(2,1)} %all-gather.11.cloned.1.call-done, bf16[2,11520,528]{1,2,0:T(8,128)(2,1)} %convert.14, bf16[128,528]{0,1:T(8,128)(2,1)S(1)} %copy-done.3), kind=kOutput, calls=%fused_computation.72 | convolution fusion | flops 1557675904 | bytes 15522368 | tf_op jit(solution)/shard_map/dot_general | solution.py:74
  290.0 19.1 %psum.7 = f32[128]{0:T(128)S(1)} all-reduce(f32[128]{0:T(128)S(1)} %get-tuple-element.25), channel_id=1, replica_groups=mesh['ra'=8,'cb'=4] {'ra'}, use_global_device_ids=true, to_apply=%region_3.4 | all-reduce | flops 128 | bytes 1024 | tf_op jit(solution)/shard_map/psum | solution.py:81
  309.0 0.8 multiply_convert_fusion
  (53 shorter events, 4.3 us)
Async XLA Ops:
  6.5 50.7 %all-gather.5.cloned.1.call-start = ((), (), s32[]{:S(2)}) async-start(), calls=%async_computation | async-start | bytes 1216512 | tf_op jit(solution)/shard_map/all_gather | solution.py:46
  7.3 140.5 %all-gather.7.cloned.1.call-start = ((), (), s32[]{:S(2)}) async-start(), calls=%async_computation.1 | async-start | bytes 3317760 | tf_op jit(solution)/shard_map/all_gather | solution.py:75
  32.2 24.9 %copy-start.7 = (f32[2,1440]{1,0:T(2,128)S(1)}, f32[2,1440]{1,0:T(2,128)}, u32[]{:S(2)}) copy-start(f32[2,1440]{1,0:T(2,128)} %param.14) | copy-start | bytes 34564
  32.2 24.9 %copy-start.8 = (f32[2,1440]{1,0:T(2,128)S(1)}, f32[2,1440]{1,0:T(2,128)}, u32[]{:S(2)}) copy-start(f32[2,1440]{1,0:T(2,128)} %param.16) | copy-start | bytes 34564
  32.2 25.0 %copy-start.6 = (f32[2,4224]{1,0:T(2,128)S(1)}, f32[2,4224]{1,0:T(2,128)}, u32[]{:S(2)}) copy-start(f32[2,4224]{1,0:T(2,128)} %param.12) | copy-start | bytes 101380
  67.3 2.9 copy-start
  67.9 15.6 %collective-permute-start = (f32[2,1440]{1,0:T(2,128)S(1)}, f32[2,1440]{1,0:T(2,128)S(1)}, u32[]{:S(2)}, u32[]{:S(2)}) collective-permute-start(f32[2,1440]{1,0:T(2,128)S(1)} %copy.12), channel_id=1, source_target_pairs={{0,1},{1,2},{2,3},{4,5},{5,6},{6,7},{8,9},{9,10},{10,11},{12,13},{... | collective-permute-start | bytes 34568 | tf_op jit(solution)/shard_map/ppermute | solution.py:14
  78.3 5.0 %copy-start.4 = (f32[2,3,1440]{2,0,1:T(2,128)S(1)}, f32[2,3,1440]{2,0,1:T(2,128)}, u32[]{:S(2)}) copy-start(f32[2,3,1440]{2,0,1:T(2,128)} %param.18) | copy-start | bytes 103684
  78.3 5.0 %copy-start.5 = (f32[2,3,1440]{2,0,1:T(2,128)S(1)}, f32[2,3,1440]{2,0,1:T(2,128)}, u32[]{:S(2)}) copy-start(f32[2,3,1440]{2,0,1:T(2,128)} %param.17) | copy-start | bytes 103684
  78.8 5.3 %collective-permute-start.1 = (f32[2,1440]{1,0:T(2,128)S(1)}, f32[2,1440]{1,0:T(2,128)S(1)}, u32[]{:S(2)}, u32[]{:S(2)}) collective-permute-start(f32[2,1440]{1,0:T(2,128)S(1)} %copy.14), channel_id=1, source_target_pairs={{0,1},{1,2},{2,3},{4,5},{5,6},{6,7},{8,9},{9,10},{10,11},{12,13},{... | collective-permute-start | bytes 34568 | tf_op jit(solution)/shard_map/ppermute | solution.py:14
  87.7 25.1 %copy-start.9 = (f32[2,528]{1,0:T(2,128)S(1)}, f32[2,528]{1,0:T(2,128)}, u32[]{:S(2)}) copy-start(f32[2,528]{1,0:T(2,128)} %param.20) | copy-start | bytes 12676
  87.7 60.0 %copy-start.2 = (bf16[128,528]{0,1:T(8,128)(2,1)S(1)}, bf16[128,528]{0,1:T(8,128)(2,1)}, u32[]{:S(2)}) copy-start(bf16[128,528]{0,1:T(8,128)(2,1)} %param.11) | copy-start | bytes 405508
  87.7 108.6 %all-gather.9.cloned.1.call-start = ((), (), s32[]{:S(2)}) async-start(), calls=%async_computation.2 | async-start | bytes 1216512 | tf_op jit(solution)/shard_map/all_gather | solution.py:46
  157.0 125.7 %all-gather.11.cloned.1.call-start = ((), (), s32[]{:S(2)}) async-start(), calls=%async_computation.3 | async-start | bytes 3317760 | tf_op jit(solution)/shard_map/all_gather | solution.py:75
  206.4 1.8 copy-start.1
  206.9 13.9 %collective-permute-start.2 = (f32[2,1440]{1,0:T(2,128)S(1)}, f32[2,1440]{1,0:T(2,128)S(1)}, u32[]{:S(2)}, u32[]{:S(2)}) collective-permute-start(f32[2,1440]{1,0:T(2,128)S(1)} %copy.16), channel_id=1, source_target_pairs={{0,1},{1,2},{2,3},{4,5},{5,6},{6,7},{8,9},{9,10},{10,11},{12,13},{... | collective-permute-start | bytes 34568 | tf_op jit(solution)/shard_map/ppermute | solution.py:14
  216.7 4.9 %collective-permute-start.3 = (f32[2,1440]{1,0:T(2,128)S(1)}, f32[2,1440]{1,0:T(2,128)S(1)}, u32[]{:S(2)}, u32[]{:S(2)}) collective-permute-start(f32[2,1440]{1,0:T(2,128)S(1)} %copy.18), channel_id=1, source_target_pairs={{0,1},{1,2},{2,3},{4,5},{5,6},{6,7},{8,9},{9,10},{10,11},{12,13},{... | collective-permute-start | bytes 34568 | tf_op jit(solution)/shard_map/ppermute | solution.py:14
  221.1 61.6 %copy-start.3 = (bf16[128,528]{0,1:T(8,128)(2,1)S(1)}, bf16[128,528]{0,1:T(8,128)(2,1)}, u32[]{:S(2)}) copy-start(bf16[128,528]{0,1:T(8,128)(2,1)} %fusion.24) | copy-start | bytes 405508
  282.7 26.3 %copy-start.10 = (f32[528]{0:T(1024)S(1)}, f32[528]{0:T(1024)}, u32[]{:S(2)}) copy-start(f32[528]{0:T(1024)} %param.21) | copy-start | bytes 6340
Sparse Core Ops, SparseCore 0:
  9.5 43.2 all-gather.4
  87.8 59.8 all-gather.6
  157.1 39.1 all-gather.8
  225.4 57.3 all-gather.10
where the time goes:
time: 317 us; the launch traced here: 316 us
  waiting for transfers between devices  133 us (42%)
  other arithmetic  85.8 us (27%)
  matrix products  48.9 us (15%)
  blocking collectives  19.1 us (6%)
  between operations  13.4 us (4%)
  starting transfers between devices  12.6 us (4%)
  local copies, waits for them, and re-layouts  3.63 us (1%)
    all_gather x2, waiting for transfers between devices, per_device(): lax.all_gather(hidden, 'ra', axis=1, tiled=True)  92.4 us
    another operation x3, other arithmetic  74.7 us
    all_gather x2, waiting for transfers between devices, per_device(): lax.all_gather(tok_rows, 'ra', axis=1, tiled=True).astype(jnp.float32)  39.1 us
    psum x1, blocking collectives, per_device(): sq_final = lax.psum(jnp.sum(wide_rows * wide_rows, axis=1), 'ra')  19.1 us
    dot_general x2, matrix products, per_device(): jnp.dot(scaled, gate_weight[layer_idx].astype(jnp.bfloat16), preferred_el...  16.5 us
    dot_general x2, matrix products, per_device(): jnp.dot(lax.all_gather(hidden, 'ra', axis=1, tiled=True), down_bf, prefer...  16.4 us
    dot_general x2, matrix products, per_device(): jnp.dot(scaled, value_weight[layer_idx].astype(jnp.bfloat16), preferred_e...  16 us
    ppermute x4, starting transfers between devices, from_behind(): return lax.ppermute(value, axis, pairs)  12.2 us
  transfers between devices with their start and end apart: 8, of which 5 were waited for; matrix products, arithmetic and copies ran while one was open for 29% of the time, Pallas kernels for 0%

commit v1 on v0

--- a/solution.py
+++ b/solution.py
@@ -43,7 +43,7 @@
     taps = gate_taps.shape[1]
     for layer_idx in range(layer_count):
         wide_rows = tok_rows.astype(jnp.float32)
-        full_rows = lax.all_gather(tok_rows, "ra", axis=1, tiled=True).astype(jnp.float32)
+        full_rows = jnp.concatenate(lax.all_gather(tok_rows, "ra"), axis=1).astype(jnp.float32)
         inv_norm = lax.rsqrt(jnp.mean(full_rows * full_rows, axis=1, keepdims=True) + epsilon)
         scaled = (full_rows * norm_gain[layer_idx]).astype(jnp.bfloat16)
         gate_pre = (

time: 317 us -> 314 us (level)
  matrix products: 48.9 us -> 41.9 us
    dot_general x2, matrix products: 16.5 us -> 12.7 us  [per_device(): jnp.dot(scaled, gate_weight[layer_idx].astype(jnp.bfloat16), preferred_el...]
    unnamed x0 -> x2, other arithmetic: none -> 3.26 us
    dot_general x2, matrix products: 16 us -> 12.7 us  [per_device(): jnp.dot(scaled, value_weight[layer_idx].astype(jnp.bfloat16), preferred_e...]
where the time goes in v1:
time: 314 us; the launch traced here: 313 us
  waiting for transfers between devices  132 us (42%)
  other arithmetic  87.5 us (28%)
  matrix products  41.9 us (13%)
  blocking collectives  19.1 us (6%)
  between operations  13.4 us (4%)
  starting transfers between devices  12.9 us (4%)
  local copies, waits for them, and re-layouts  5.85 us (2%)
    all_gather x2, waiting for transfers between devices, per_device(): lax.all_gather(hidden, 'ra', axis=1, tiled=True)  92.5 us
    another operation x3, other arithmetic  74.7 us
    all_gather x2, waiting for transfers between devices, per_device(): lax.all_gather(tok_rows, 'ra')  38.3 us
    psum x1, blocking collectives, per_device(): sq_final = lax.psum(jnp.sum(wide_rows * wide_rows, axis=1), 'ra')  19.1 us
    dot_general x2, matrix products, per_device(): jnp.dot(lax.all_gather(hidden, 'ra', axis=1, tiled=True), down_bf, prefer...  16.4 us
    dot_general x2, matrix products, per_device(): jnp.dot(scaled, value_weight[layer_idx].astype(jnp.bfloat16), preferred_e...  12.7 us
    dot_general x2, matrix products, per_device(): jnp.dot(scaled, gate_weight[layer_idx].astype(jnp.bfloat16), preferred_el...  12.7 us
    ppermute x4, starting transfers between devices, from_behind(): return lax.ppermute(value, axis, pairs)  12.7 us
  transfers between devices with their start and end apart: 8, of which 5 were waited for; matrix products, arithmetic and copies ran while one was open for 29% of the time, Pallas kernels for 0%

profile of v1, /device:TPU:0, one launch (start us, length us, event | category | flops | bytes accessed | tf_op | source)
XLA Modules:
  0.0 313.0 jit_solution(1750459362190542594)
XLA Ops:
  7.3 0.9 slice_reduce_fusion
  8.5 24.8 %convert.13 = bf16[2,4224,1440]{1,2,0:T(8,128)(2,1)} convert(f32[2,4224,1440]{1,2,0:T(8,128)} %param.15) | non-fusion elementwise | flops 12165120 | bytes 72990720 | tf_op jit(solution)/shard_map/convert.4
  33.3 24.9 %convert.12 = bf16[2,4224,1440]{1,2,0:T(8,128)(2,1)} convert(f32[2,4224,1440]{1,2,0:T(8,128)} %param.13) | non-fusion elementwise | flops 12165120 | bytes 72990720 | tf_op jit(solution)/shard_map/convert.5
  58.3 1.5 convert_bitcast_fusion.2
  61.2 6.4 %fusion.12 = f32[128,1440]{0,1:T(8,128)S(1)} fusion(bf16[128,4224]{0,1:T(8,128)(2,1)S(1)} %bitcast.89, bf16[2,4224,1440]{1,2,0:T(8,128)(2,1)} %convert.13, f32[1440]{0:T(1024)S(1)} %get-tuple-element.22, f32[128]{0:T(128)S(1)} %add_rsqrt_fusion.2), kind=kOutput, calls=%fused_computation.20 | convolution fusion | flops 1557504000 | bytes 13990016 | tf_op jit(solution)/shard_map/dot_general | solution.py:59
  68.1 2.4 collective-permute-start.1
  70.5 6.4 %fusion.13 = f32[128,1440]{0,1:T(8,128)S(1)} fusion(bf16[128,4224]{0,1:T(8,128)(2,1)S(1)} %bitcast.90, bf16[2,4224,1440]{1,2,0:T(8,128)(2,1)} %convert.12, f32[1440]{0:T(1024)S(1)} %get-tuple-element.20, f32[128]{0:T(128)S(1)} %add_rsqrt_fusion.2), kind=kOutput, calls=%fused_computation.21 | convolution fusion | flops 1557504000 | bytes 13990016 | tf_op jit(solution)/shard_map/dot_general | solution.py:50
  77.4 4.6 %collective-permute-start = (f32[2,1440]{1,0:T(2,128)S(1)}, f32[2,1440]{1,0:T(2,128)S(1)}, u32[]{:S(2)}, u32[]{:S(2)}) collective-permute-start(f32[2,1440]{1,0:T(2,128)S(1)} %copy.20), channel_id=1, source_target_pairs={{0,1},{1,2},{2,3},{4,5},{5,6},{6,7},{8,9},{9,10},{10,11},{12,13},{... | collective-permute-start | bytes 34568 | tf_op jit(solution)/shard_map/ppermute | solution.py:14
  83.1 3.3 %fusion.40 = bf16[128,1440]{0,1:T(8,128)(2,1)} fusion(f32[2,1440]{0,1:T(8,128)S(1)} %copy.23, f32[128,1440]{0,1:T(8,128)S(1)} %fusion.12, f32[128,1440]{0,1:T(8,128)S(1)} %fusion.13, f32[2,1440]{0,1:T(8,128)S(1)} %copy.21, f32[1440]{0:T(1024)S(1)} %get-tuple-element.12, f32[1440]{0:T(1024)S(1)} %get-tuple-element.13, f32[1440]{0:T(1024)S(1)} %get-tuple-element.14, ...), kind=kLoop, calls=%fused_computation.61 | loop fusion | flops 3686400 | bytes 1900800 | tf_op jit(solution)/shard_map/convert_element_type | solution.py:73
  86.5 25.0 %convert.14 = bf16[2,11520,528]{1,2,0:T(8,128)(2,1)} convert(f32[2,11520,528]{1,2,0:T(8,128)} %param.19) | non-fusion elementwise | flops 12165120 | bytes 72990720 | tf_op jit(solution)/shard_map/convert.3
  111.5 34.9 %all-gather.7.cloned.1.call-done = bf16[128,11520]{0,1:T(8,128)(2,1)} async-done(((bf16[128,1440]{0,1:T(8,128)(2,1)}), bf16[128,11520]{0,1:T(8,128)(2,1)}) %all-gather.7.cloned.1.call-update) | async-done | bytes 2949136 | tf_op jit(solution)/shard_map/all_gather | solution.py:75
  146.4 9.3 %fusion.24 = bf16[128,528]{0,1:T(8,128)(2,1)} fusion(bf16[128,11520]{0,1:T(8,128)(2,1)} %all-gather.7.cloned.1.call-done, bf16[2,11520,528]{1,2,0:T(8,128)(2,1)} %convert.14, bf16[128,528]{0,1:T(8,128)(2,1)S(1)} %copy-done, f32[528]{0:T(1024)S(1)} %get-tuple-element.24), kind=kOutput, calls=%fused_computation.45 | convolution fusion | flops 1557473280 | bytes 15386688 | tf_op jit(solution)/shard_map/dot_general | solution.py:74
  155.8 38.3 %all-gather.13.cloned.1.call-done = bf16[1024,528]{0,1:T(8,128)(2,1)} async-done(((bf16[128,528]{0,1:T(8,128)(2,1)}), bf16[1024,528]{0,1:T(8,128)(2,1)}) %all-gather.13.cloned.1.call-update) | async-done | bytes 1081360 | tf_op jit(solution)/shard_map/all_gather | solution.py:46
  194.1 1.8 convert_bitcast_fusion.1
  197.0 0.8 fusion.17
  197.7 6.4 %fusion.10 = f32[128,1440]{0,1:T(8,128)S(1)} fusion(bf16[128,4224]{0,1:T(8,128)(2,1)S(1)} %bitcast.87, bf16[2,4224,1440]{1,2,0:T(8,128)(2,1)} %convert.13, f32[1440]{0:T(1024)S(1)} %get-tuple-element.21, f32[128]{0:T(128)S(1)} %add_rsqrt_fusion.1), kind=kOutput, calls=%fused_computation.18 | convolution fusion | flops 1557504000 | bytes 13990016 | tf_op jit(solution)/shard_map/dot_general | solution.py:59
  204.6 1.5 collective-permute-start.3
  206.1 6.4 %fusion.11 = f32[128,1440]{0,1:T(8,128)S(1)} fusion(bf16[128,4224]{0,1:T(8,128)(2,1)S(1)} %bitcast.88, bf16[2,4224,1440]{1,2,0:T(8,128)(2,1)} %convert.12, f32[1440]{0:T(1024)S(1)} %get-tuple-element.19, f32[128]{0:T(128)S(1)} %add_rsqrt_fusion.1), kind=kOutput, calls=%fused_computation.19 | convolution fusion | flops 1557504000 | bytes 13990016 | tf_op jit(solution)/shard_map/dot_general | solution.py:50
  213.0 4.3 %collective-permute-start.2 = (f32[2,1440]{1,0:T(2,128)S(1)}, f32[2,1440]{1,0:T(2,128)S(1)}, u32[]{:S(2)}, u32[]{:S(2)}) collective-permute-start(f32[2,1440]{1,0:T(2,128)S(1)} %copy.25), channel_id=1, source_target_pairs={{0,1},{1,2},{2,3},{4,5},{5,6},{6,7},{8,9},{9,10},{10,11},{12,13},{... | collective-permute-start | bytes 34568 | tf_op jit(solution)/shard_map/ppermute | solution.py:14
  218.4 3.3 %fusion.30 = bf16[128,1440]{0,1:T(8,128)(2,1)} fusion(f32[2,1440]{0,1:T(8,128)S(1)} %copy.28, f32[128,1440]{0,1:T(8,128)S(1)} %fusion.10, f32[128,1440]{0,1:T(8,128)S(1)} %fusion.11, f32[2,1440]{0,1:T(8,128)S(1)} %copy.26, f32[1440]{0:T(1024)S(1)} %get-tuple-element.15, f32[1440]{0:T(1024)S(1)} %get-tuple-element.16, f32[1440]{0:T(1024)S(1)} %get-tuple-element.11, ...), kind=kLoop, calls=%fused_computation.51 | loop fusion | flops 3686400 | bytes 1900800 | tf_op jit(solution)/shard_map/convert_element_type | solution.py:73
  221.8 57.6 %all-gather.9.cloned.1.call-done = bf16[128,11520]{0,1:T(8,128)(2,1)} async-done(((bf16[128,1440]{0,1:T(8,128)(2,1)}), bf16[128,11520]{0,1:T(8,128)(2,1)}) %all-gather.9.cloned.1.call-update) | async-done | bytes 2949136 | tf_op jit(solution)/shard_map/all_gather | solution.py:75
  279.3 7.2 %multiply_reduce_fusion = (f32[128]{0:T(128)S(1)}, f32[128,528]{0,1:T(8,128)S(1)}) fusion(f32[528]{0:T(1024)S(1)} %get-tuple-element.23, bf16[128,11520]{0,1:T(8,128)(2,1)} %all-gather.9.cloned.1.call-done, bf16[2,11520,528]{1,2,0:T(8,128)(2,1)} %convert.14, bf16[128,528]{0,1:T(8,128)(2,1)S(1)} %copy-done.1), kind=kOutput, calls=%fused_computation.75 | convolution fusion | flops 1557675904 | bytes 15522368 | tf_op jit(solution)/shard_map/dot_general | solution.py:74
  286.5 19.1 %psum.7 = f32[128]{0:T(128)S(1)} all-reduce(f32[128]{0:T(128)S(1)} %get-tuple-element.29), channel_id=1, replica_groups=mesh['ra'=8,'cb'=4] {'ra'}, use_global_device_ids=true, to_apply=%region_3.4 | all-reduce | flops 128 | bytes 1024 | tf_op jit(solution)/shard_map/psum | solution.py:81
  305.6 0.8 multiply_convert_fusion
  (56 shorter events, 8.0 us)
Async XLA Ops:
  6.5 51.7 %all-gather.11.cloned.1.call-start = ((), (), s32[]{:S(2)}) async-start(), calls=%async_computation.2 | async-start | bytes 1216512 | tf_op jit(solution)/shard_map/all_gather | solution.py:46
  7.3 139.2 %all-gather.7.cloned.1.call-start = ((), (), s32[]{:S(2)}) async-start(), calls=%async_computation | async-start | bytes 3317760 | tf_op jit(solution)/shard_map/all_gather | solution.py:75
  33.3 24.9 %copy-start.4 = (f32[2,1440]{1,0:T(2,128)S(1)}, f32[2,1440]{1,0:T(2,128)}, u32[]{:S(2)}) copy-start(f32[2,1440]{1,0:T(2,128)} %param.16) | copy-start | bytes 34564
  33.3 24.9 %copy-start.5 = (f32[2,1440]{1,0:T(2,128)S(1)}, f32[2,1440]{1,0:T(2,128)}, u32[]{:S(2)}) copy-start(f32[2,1440]{1,0:T(2,128)} %param.14) | copy-start | bytes 34564
  68.1 14.1 %collective-permute-start.1 = (f32[2,1440]{1,0:T(2,128)S(1)}, f32[2,1440]{1,0:T(2,128)S(1)}, u32[]{:S(2)}, u32[]{:S(2)}) collective-permute-start(f32[2,1440]{1,0:T(2,128)S(1)} %copy.22), channel_id=1, source_target_pairs={{0,1},{1,2},{2,3},{4,5},{5,6},{6,7},{8,9},{9,10},{10,11},{12,13},{... | collective-permute-start | bytes 34568 | tf_op jit(solution)/shard_map/ppermute | solution.py:14
  76.9 5.1 %copy-start.2 = (f32[2,3,1440]{2,0,1:T(2,128)S(1)}, f32[2,3,1440]{2,0,1:T(2,128)}, u32[]{:S(2)}) copy-start(f32[2,3,1440]{2,0,1:T(2,128)} %param.18) | copy-start | bytes 103684
  76.9 5.1 %copy-start.3 = (f32[2,3,1440]{2,0,1:T(2,128)S(1)}, f32[2,3,1440]{2,0,1:T(2,128)}, u32[]{:S(2)}) copy-start(f32[2,3,1440]{2,0,1:T(2,128)} %param.17) | copy-start | bytes 103684
  77.4 5.4 %collective-permute-start = (f32[2,1440]{1,0:T(2,128)S(1)}, f32[2,1440]{1,0:T(2,128)S(1)}, u32[]{:S(2)}, u32[]{:S(2)}) collective-permute-start(f32[2,1440]{1,0:T(2,128)S(1)} %copy.20), channel_id=1, source_target_pairs={{0,1},{1,2},{2,3},{4,5},{5,6},{6,7},{8,9},{9,10},{10,11},{12,13},{... | collective-permute-start | bytes 34568 | tf_op jit(solution)/shard_map/ppermute | solution.py:14
  86.4 25.1 %copy-start.6 = (f32[2,528]{1,0:T(2,128)S(1)}, f32[2,528]{1,0:T(2,128)}, u32[]{:S(2)}) copy-start(f32[2,528]{1,0:T(2,128)} %param.20) | copy-start | bytes 12676
  86.4 60.0 %copy-start = (bf16[128,528]{0,1:T(8,128)(2,1)S(1)}, bf16[128,528]{0,1:T(8,128)(2,1)}, u32[]{:S(2)}) copy-start(bf16[128,528]{0,1:T(8,128)(2,1)} %param.11) | copy-start | bytes 405508
  86.4 107.7 %all-gather.13.cloned.1.call-start = ((), (), s32[]{:S(2)}) async-start(), calls=%async_computation.3 | async-start | bytes 1216512 | tf_op jit(solution)/shard_map/all_gather | solution.py:46
  155.7 123.6 %all-gather.9.cloned.1.call-start = ((), (), s32[]{:S(2)}) async-start(), calls=%async_computation.1 | async-start | bytes 3317760 | tf_op jit(solution)/shard_map/all_gather | solution.py:75
  204.6 12.7 %collective-permute-start.3 = (f32[2,1440]{1,0:T(2,128)S(1)}, f32[2,1440]{1,0:T(2,128)S(1)}, u32[]{:S(2)}, u32[]{:S(2)}) collective-permute-start(f32[2,1440]{1,0:T(2,128)S(1)} %copy.27), channel_id=1, source_target_pairs={{0,1},{1,2},{2,3},{4,5},{5,6},{6,7},{8,9},{9,10},{10,11},{12,13},{... | collective-permute-start | bytes 34568 | tf_op jit(solution)/shard_map/ppermute | solution.py:14
  213.0 5.1 %collective-permute-start.2 = (f32[2,1440]{1,0:T(2,128)S(1)}, f32[2,1440]{1,0:T(2,128)S(1)}, u32[]{:S(2)}, u32[]{:S(2)}) collective-permute-start(f32[2,1440]{1,0:T(2,128)S(1)} %copy.25), channel_id=1, source_target_pairs={{0,1},{1,2},{2,3},{4,5},{5,6},{6,7},{8,9},{9,10},{10,11},{12,13},{... | collective-permute-start | bytes 34568 | tf_op jit(solution)/shard_map/ppermute | solution.py:14
  217.6 61.7 %copy-start.1 = (bf16[128,528]{0,1:T(8,128)(2,1)S(1)}, bf16[128,528]{0,1:T(8,128)(2,1)}, u32[]{:S(2)}) copy-start(bf16[128,528]{0,1:T(8,128)(2,1)} %fusion.24) | copy-start | bytes 405508
  279.3 26.3 %copy-start.7 = (f32[528]{0:T(1024)S(1)}, f32[528]{0:T(1024)}, u32[]{:S(2)}) copy-start(f32[528]{0:T(1024)} %param.21) | copy-start | bytes 6340
Sparse Core Ops, SparseCore 0:
  9.4 42.3 all-gather.10
  86.5 59.8 all-gather.6
  155.8 38.2 all-gather.12
  221.9 57.4 all-gather.8
